TPU v7x, 32 devices: a whole 2x2x4 slice. The times are simulated.
32 devices in a mesh: sp: 4 (over y, x), dp: 8 (over z, core).
Axes of the slice: x: 2, y: 2, z: 4, core: 2. Of those that a mesh axis runs over, the one named last changes fastest.
Arguments:
- tokens: bfloat16 [8, 1280, 2048], P('dp', 'sp'), may hold values from -6 to 6
- up_weight: bfloat16 [2048, 2048], P('dp'), may hold values from -0.125 to 0.125
- gate_weight: bfloat16 [2048, 2048], P('dp'), may hold values from -0.125 to 0.125
- group_gain: float32 [16, 128], P('sp'), may hold values from 0.1 to 1.9
- mix_weight: bfloat16 [16, 1280, 1280], P('sp', 'dp'), may hold values from -0.15625 to 0.15625
- mix_bias: float32 [16, 1280], P('sp'), may hold values from 0.5 to 1.5
- out_gain: float32 [2048], replicated, may hold values from 0.1 to 1.9
- out_weight: bfloat16 [2048, 2048], P(None, 'dp'), may hold values from -0.125 to 0.125
Outputs:
- mixed_out: bfloat16 [8, 1280, 2048], P('dp', 'sp')
All inputs are finite; a program needn't handle non-finite values.
Results may differ from a plain program's by a relative error of at most 0.0072.
Values may be sent and summed in bfloat16 or wider, within the bound.
A program may use at most 128 MiB of HBM per device.

v0:
```python
import functools

import jax
import jax.numpy as jnp
from jax import lax
from jax.experimental import pallas as pl
from jax.experimental.pallas import tpu as pltpu
from jax.sharding import PartitionSpec as P

norm_eps = 1e-06
CORES = 2
LANES = 128
MESH = pl.DeviceIdType.MESH


def up_to(n, m):
    return -(-n // m) * m


def fused_kernel(
    sp, zs,
    tok_ref, up_ref, gate_ref, gain_ref, mix_ref, bias_ref, ogain_ref, outw_ref, out_ref,
    tok_v, ug_v, mix_v, outw_v, open_v, norm_v, other_v, bias_v, mixed_v, gated_v, held_v,
    normed_v, sums_v, part_v,
    load_sem,
    ug_line, ug_up, ug_dn, ug_ps, ug_pr,
    ow_line, ow_up, ow_dn, ow_ps, ow_pr, pl_s, pl_r, pp_s, pp_r,
    mx_line, mx_up, mx_dn, mx_ps, mx_pr,
    tok_s, tok_r, v_s, v_r, ret_s, ret_r, ga_s, ga_r,
):
    me = lax.axis_index("sp")
    dp = lax.axis_index("dp")
    z, c = dp // CORES, lax.rem(dp, CORES)
    groups, dps, rows, block = mix_v.shape
    per, width = out_ref.shape
    gd = gain_ref.shape[2]
    chans = groups * gd
    depth, ncol = up_ref.shape[0], outw_ref.shape[1]
    total = sp * per
    blocks = total // block
    parts, _, pk, _ = outw_v.shape
    zr = CORES * rows
    half, dhalf = per // 2, depth // 2
    square = sp == 4

    partner = {"dp": z * CORES + (1 - c)}

    def at_line(zz):
        return {"dp": zz * CORES + c}

    def around(r, sign):
        if square:
            y = lax.rem(me // 2 + r // 2, 2)
            x = lax.rem(lax.rem(me, 2) + r % 2, 2)
            return y * 2 + x
        return lax.rem(me + sign * r + sp, sp)

    def target(r):
        return around(r, 1)

    def source(r):
        return around(r, -1)

    def peer(r):
        return {"sp": target(r)}

    def inner(zz):
        return 0 < zz < zs - 1

    def mate(zz):
        return {0: 1, 1: 0, zs - 1: zs - 2, zs - 2: zs - 1}.get(zz)

    def remote(src, dst, send, recv, device):
        return pltpu.make_async_remote_copy(
            src_ref=src, dst_ref=dst, send_sem=send, recv_sem=recv,
            device_id=device, device_id_type=MESH)

    def arrived(ref, sem):
        remote(ref, ref, sem, sem, partner).wait_recv()

    def each_z(fn, only=None):
        for zz in range(zs):
            if only is None or only(zz):
                pl.when(z == zz)(functools.partial(fn, zz))

    def each_d(fn, only=None):
        for zz in range(zs):
            if only is None or only(zz):
                for cc in range(CORES):
                    pl.when(dp == zz * CORES + cc)(functools.partial(fn, zz, cc))

    loads = {"ug": [], "tok": [], "ow": [], "mx": []}
    for g in range(groups):
        for t, ref in enumerate((up_ref, gate_ref)):
            cols = pl.ds(pl.multiple_of(me * chans + g * gd, LANES), gd)
            spot = 2 * g + t
            loads["ug"].append(pltpu.make_async_copy(
                ref.at[:, cols],
                ug_v.at[pl.ds(dp * depth, depth), pl.ds(spot * gd, gd)],
                load_sem.at[3 + spot]))
    loads["tok"].append(pltpu.make_async_copy(tok_ref, tok_v.at[me], load_sem.at[0]))
    for p in range(parts):
        loads["ow"].append(pltpu.make_async_copy(
            outw_ref.at[pl.ds(me * chans + p * pk, pk), :],
            outw_v.at[p, me, :, pl.ds(pl.multiple_of(dp * ncol, LANES), ncol)],
            load_sem.at[3 + 2 * groups + p]))
    loads["mx"].append(pltpu.make_async_copy(mix_ref, mix_v.at[:, dp], load_sem.at[2]))
    for kind in ("ug", "tok", "ow", "mx"):
        for load in loads[kind]:
            load.start()

    barrier = pltpu.get_barrier_semaphore()

    def greet(zz):
        friends = [partner] + [peer(r) for r in range(1, sp)]
        if zz > 0:
            friends.append(at_line(zz - 1))
        if zz < zs - 1:
            friends.append(at_line(zz + 1))
        for friend in friends:
            pl.semaphore_signal(barrier, inc=1, device_id=friend, device_id_type=MESH)
        pl.semaphore_wait(barrier, len(friends))

    each_z(greet)

    def ug_piece(o, cc, h):
        return ug_v.at[pl.ds((o * CORES + cc) * depth + h * dhalf, dhalf), :]

    def ow_piece(s, o, cc):
        cols = pl.ds(pl.multiple_of((o * CORES + cc) * ncol, LANES), ncol)
        return outw_v.at[:, s, :, cols]

    def cuts(d):
        out, at, end = [], d * rows, (d + 1) * rows
        while at < end:
            top = min(end, (at // LANES + 1) * LANES)
            out.append((at - d * rows, top - at, min(block, up_to(top, LANES))))
            at = top
        return out

    def mx_piece(g, d, piece):
        r0, rn, cols = piece
        return mix_v.at[g, d, pl.ds(r0, rn), pl.ds(0, cols)]

    def ug_copies(zz, o, h):
        src, out = ug_piece(o, c, h), []
        if o >= zz and zz > 0:
            out.append(remote(src, src, ug_dn.at[o, h], ug_line.at[o, h], at_line(zz - 1)))
        if o <= zz and zz < zs - 1:
            out.append(remote(src, src, ug_up.at[o, h], ug_line.at[o, h], at_line(zz + 1)))
        out.append(remote(src, src, ug_ps.at[o, h], ug_pr.at[o, h], partner))
        return out

    def ow_down(zz, o):
        src = ow_piece(me, o, c)
        if o >= zz and zz > 0:
            return [remote(src, src, ow_dn.at[o], ow_line.at[o], at_line(zz - 1))]
        return []

    def ow_rise(zz, o):
        src = ow_piece(me, o, c)
        if o <= zz and zz < zs - 1:
            return [remote(src, src, ow_up.at[o], ow_line.at[o], at_line(zz + 1))]
        return []

    def ow_pair(o):
        src = ow_piece(me, o, c)
        return [remote(src, src, ow_ps.at[o], ow_pr.at[o], partner)]

    def mx_copies(zz, cc, g, o, way):
        out = []
        d = o * CORES + cc
        for i, piece in enumerate(cuts(d)):
            src = mx_piece(g, d, piece)
            if way == "dn" and o >= zz and inner(zz - 1):
                out.append(remote(src, src, mx_dn.at[g, o, i], mx_line.at[g, o, i], at_line(zz - 1)))
            if way == "up" and o <= zz and inner(zz + 1):
                out.append(remote(src, src, mx_up.at[g, o, i], mx_line.at[g, o, i], at_line(zz + 1)))
            if way == "pair" and (inner(zz) or o == zz):
                out.append(remote(src, src, mx_ps.at[g, o, i], mx_pr.at[g, o, i], partner))
        return out

    def go(copies):
        for copy in copies:
            copy.start()

    def own_mix(zz, way, low=0, high=groups):
        for cc in range(CORES):
            @pl.when(c == cc)
            def _():
                @pl.loop(low, high)
                def _(g):
                    go(mx_copies(zz, cc, g, zz, way))

    def ug_left(zz, way, k):
        far = zs - 1 - zz if way == "dn" else zz
        there = zz > 0 if way == "dn" else zz < zs - 1
        return there, max(0, far - k)

    held_back = max(1, groups - 1)

    def own_out(zz, way):
        go(ow_down(zz, zz) if way == "dn" else ow_rise(zz, zz))

    for load in loads["ug"]:
        load.wait()

    def first_weights(zz):
        for h in range(2):
            go(ug_copies(zz, zz, h))

    each_z(first_weights)
    for load in loads["tok"]:
        load.wait()

    def tok_half(s, h):
        return tok_v.at[s, pl.ds(h * half, half), :]

    def tok_copy(s, r, h, r_there):
        return remote(tok_half(s, h), tok_half(s, h), tok_s.at[r_there, h], tok_r.at[r_there, h], peer(r))

    def tok_first():
        if square:
            return [tok_copy(me, 1, 0, 1), tok_copy(me, 2, 1, 2), tok_copy(me, 1, 1, 1), tok_copy(me, 2, 0, 2)]
        return [tok_copy(me, r, h, r) for r in range(1, sp) for h in range(2)]

    def tok_second():
        if square:
            return [tok_copy(source(1), 2, 0, 3), tok_copy(source(2), 1, 1, 3)]
        return []

    go(tok_first())
    for load in loads["ow"] + loads["mx"]:
        load.wait()

    def first_rest(zz):
        go(ow_pair(zz))
        for way in ("dn", "up"):
            there, left = ug_left(zz, way, 0)
            if there and left == 0:
                own_out(zz, way)
                own_mix(zz, way, 0, held_back if zz == zs - 1 else groups)
        own_mix(zz, "pair")

    each_z(first_rest)

    for g in range(groups):
        for t in range(block // LANES):
            spot = slice(t * LANES, (t + 1) * LANES)
            bias_v[g, spot, :] = jnp.broadcast_to(bias_ref[g:g + 1, spot], (gd, LANES)).T

    def take_ug(zz, k):
        for o in (zz + k, zz - k):
            if 0 <= o < zs:
                for h in range(2):
                    arrived(ug_piece(o, c, h), ug_line.at[o, h])
                    go(ug_copies(zz, o, h))
        for way in ("dn", "up"):
            there, left = ug_left(zz, way, k)
            before = ug_left(zz, way, k - 1)[1]
            if there and left == 0 and before > 0:
                own_out(zz, way)
                own_mix(zz, way, 0, 1)

    def take_out(zz, k):
        for o in (zz + k, zz - k):
            if 0 <= o < zs:
                arrived(ow_piece(me, o, c), ow_line.at[o])
                go(ow_down(zz, o) if o > zz else ow_rise(zz, o))
                go(ow_pair(o))
        for way in ("dn", "up"):
            there, left = ug_left(zz, way, k)
            before = ug_left(zz, way, k - 1)[1]
            if there and left == 0 and before > 0:
                own_mix(zz, way, 1, groups)

    def plane_first(o):
        src = ow_piece(me, o, c)
        reach = (1, 2) if square else range(1, sp)
        return [remote(src, src, pl_s.at[r, o], pl_r.at[r, o], peer(r)) for r in reach]

    def plane_second(o):
        if not square:
            return []
        via, to = (1, 2) if o < zs // 2 else (2, 1)
        src = ow_piece(source(via), o, c)
        return [remote(src, src, pl_s.at[3, o], pl_r.at[3, o], peer(to))]

    def plane_pair(r, o):
        src = ow_piece(source(r), o, c)
        return [remote(src, src, pp_s.at[r, o], pp_r.at[r, o], partner)]

    each_z(lambda zz: take_ug(zz, 1))
    if square:
        arrived(tok_half(source(1), 0), tok_r.at[1, 0])
        arrived(tok_half(source(2), 1), tok_r.at[2, 1])
    go(tok_second())

    def more_weights(zz):
        for k in range(2, zs):
            take_ug(zz, k)
        if inner(zz) and not square:
            for k in range(1, zs):
                take_out(zz, k)
            for o in range(zs):
                go(plane_first(o))
        if not inner(zz):
            go(plane_first(zz))

    each_z(more_weights)

    def weights_in(zz):
        for o in range(zs):
            for h in range(2):
                arrived(ug_piece(o, 1 - c, h), ug_pr.at[o, h])

    weights_in(None)

    def v_copy(zz, q):
        spot = pl.ds(pl.multiple_of(q * per, 16), per)
        return remote(norm_v.at[:, spot, :], other_v.at[:, spot, :],
                      v_s.at[q], v_r.at[q], at_line(mate(zz)))

    def starts(q):
        return (q * per) % block

    def v_useful(end, q):
        return any(starts(q) < (o + 1) * zr for o in range(zs) if o != end) or block % per > 0

    def send_v(zz, s):
        for q in range(sp):
            if v_useful(zz, q):
                pl.when(s == q)(lambda q=q: v_copy(zz, q).start())

    def project(s):
        spot = pl.ds(pl.multiple_of(s * per, 16), per)

        @pl.loop(0, groups)
        def _(g):
            cols = pl.ds(pl.multiple_of(g * 2 * gd, 2 * gd), 2 * gd)
            both = jnp.dot(tok_v[s], ug_v[:, cols], preferred_element_type=jnp.float32)
            both = jax.nn.gelu(both.astype(jnp.bfloat16).astype(jnp.float32))
            open_v[g, spot, :] = both[:, :gd]
            act = both[:, gd:]
            act = act - jnp.mean(act, axis=-1, keepdims=True)
            spread = jnp.mean(act * act, axis=-1, keepdims=True)
            norm_v[g, spot, :] = (
                act * lax.rsqrt(spread + norm_eps) * gain_ref[g]
            ).astype(jnp.bfloat16)

        each_z(lambda zz: send_v(zz, s), lambda zz: not inner(zz))

    def out_events(zz, ks):
        for k in ks:
            take_out(zz, k)
            for o in (zz + k, zz - k):
                if 0 <= o < zs:
                    go(plane_first(o))
            if inner(zz) and k == 1:
                go(plane_first(zz))

    if square:
        for r in range(sp):
            for h in range(2 if r else 0):
                if r != 1 + h:
                    arrived(tok_half(source(r), h), tok_r.at[r, h])
            project(source(r))

            def events(zz, r=r):
                first = r + 1 if inner(zz) else r
                ks = range(first, zs if r == sp - 1 else first + 1)
                out_events(zz, [k for k in ks if 0 < k < zs])

            each_z(events)
    else:
        @pl.loop(0, sp)
        def _(r):
            @pl.when(r > 0)
            def _():
                for h in range(2):
                    arrived(tok_half(source(r), h), tok_r.at[r, h])

            project(source(r))

        each_z(lambda zz: out_events(zz, range(1, zs)), lambda zz: not inner(zz))

    if held_back < groups:
        each_z(lambda zz: own_mix(zz, "dn", held_back, groups), lambda zz: zz == zs - 1)

    def take_mix(zz, cc, g, o):
        d = o * CORES + cc
        for i, piece in enumerate(cuts(d)):
            arrived(mx_piece(g, d, piece), mx_line.at[g, o, i])
        go(mx_copies(zz, cc, g, o, "dn" if o > zz else "up"))
        go(mx_copies(zz, cc, g, o, "pair"))

    def passed_on(zz, o):
        return abs(o - zz) == 1 and inner(zz - 1 if o > zz else zz + 1)

    def late(zz, o):
        return zz == zs - 2 and o == zs - 1

    def near_mix(zz, cc):
        for o in (zz + 1, zz - 1):
            if passed_on(zz, o):
                @pl.loop(0, held_back if late(zz, o) else groups)
                def _(g):
                    take_mix(zz, cc, g, o)

    def late_mix(zz, cc):
        @pl.loop(held_back, groups)
        def _(g):
            take_mix(zz, cc, g, zz + 1)

    each_d(near_mix, inner)

    def ready_at(q):
        if block % per:
            return zs - 1
        return (((q + 1) * per - 1) % block) // zr

    def needs(o):
        return min(block, up_to((o + 1) * zr, LANES))

    def first_need(zz, q):
        if not v_useful(mate(zz), q):
            return None
        return next(o for o in range(zs) if o != mate(zz) and (block % per or starts(q) < needs(o)))

    def with_mate(zz, o):
        return inner(zz) and mate(zz) is not None and mate(zz) != o

    def alone(zz, o):
        return zz == o if not inner(zz) else not with_mate(zz, o)

    def gated_copy(g, q):
        return remote(gated_v.at[g, pl.ds(q * per, per), :], held_v.at[me, g],
                      ga_s.at[g, q], ga_r.at[g, me], {"sp": q})

    def ret_copy(zz, g, o):
        spot = mixed_v.at[g, :, o]
        return remote(spot, spot, ret_s.at[g, o], ret_r.at[g, o], at_line(mate(zz)))

    def hand_over(g, o):
        for q in range(sp):
            if ready_at(q) == o:
                @pl.when(me == q)
                def _():
                    held_v[q, g] = gated_v[g, pl.ds(q * per, per), :]

                @pl.when(me != q)
                def _():
                    gated_copy(g, q).start()

    def one_of(zs_in):
        return functools.reduce(jnp.logical_or, [z == zz for zz in zs_in])

    def clear_unsent(zz):
        for q in range(sp):
            if not v_useful(mate(zz), q):
                high = max(needs(o) for o in range(zs) if o != mate(zz)) - starts(q)
                if high > 0:
                    other_v[:, q * per:q * per + high, :] = jnp.zeros(
                        (groups, high, gd), jnp.bfloat16)

    each_z(clear_unsent, lambda zz: inner(zz) and mate(zz) is not None)

    def unit(o, low=0, high=groups, only=None, but=None):
        lo = o * zr
        base, top = lo // LANES * LANES, needs(o)

        def wait_v(zz):
            for q in range(sp):
                if first_need(zz, q) == o:
                    arrived(other_v.at[:, pl.ds(q * per, per), :], v_r.at[q])

        if low == 0:
            each_z(wait_v, lambda zz: with_mate(zz, o))

        def mix(members, paired):
            @pl.loop(low, high)
            def _(g):
                def rows_in(zz, cc):
                    if o != zz and not passed_on(zz, o):
                        take_mix(zz, cc, g, o)
                    d = o * CORES + 1 - cc
                    for i, piece in enumerate(cuts(d)):
                        arrived(mx_piece(g, d, piece), mx_pr.at[g, o, i])

                def values(at, end):
                    own = norm_v[g, at:end, :]
                    return jnp.concatenate([own, other_v[g, at:end, :]], axis=1) if paired else own

                each_d(rows_in, lambda zz: zz in members)
                corner = mix_v[g, o * CORES:(o + 1) * CORES, :, base:top].reshape(zr, top - base)
                keep = lax.broadcasted_iota(jnp.int32, corner.shape, 0) + (lo - base) >= (
                    lax.broadcasted_iota(jnp.int32, corner.shape, 1))
                corner = jnp.where(keep, corner.astype(jnp.float32), 0.0).astype(jnp.bfloat16)
                bias = bias_v[g, lo:lo + zr, :]
                for b in range(blocks):
                    at = b * block
                    mixed = jnp.dot(corner, values(at + base, at + top),
                                    preferred_element_type=jnp.float32)
                    if base > 0:
                        left = mix_v[g, o * CORES:(o + 1) * CORES, :, :base].reshape(zr, base)
                        mixed += jnp.dot(left, values(at, at + base),
                                         preferred_element_type=jnp.float32)
                    spot = slice(at + lo, at + lo + zr)
                    if paired:
                        mixed_v[g, b, o] = (mixed[:, gd:] + bias).astype(jnp.bfloat16)
                    gated_v[g, spot, :] = (
                        open_v[g, spot, :] * (mixed[:, :gd] + bias)).astype(jnp.bfloat16)
                if paired:
                    each_z(lambda zz: ret_copy(zz, g, o).start(), lambda zz: zz in members)
                hand_over(g, o)

        for paired, test in ((True, with_mate), (False, alone)):
            members = [zz for zz in range(zs) if test(zz, o) and zz != but and only in (None, zz)]
            if members:
                pl.when(one_of(members))(functools.partial(mix, members, paired))

        if only is not None:
            return

        @pl.when(one_of([zz for zz in (0, zs - 1) if zz != o]))
        def _():
            @pl.loop(low, high)
            def _(g):
                arrived(mixed_v.at[g, :, o], ret_r.at[g, o])
                for b in range(blocks):
                    spot = slice(b * block + lo, b * block + lo + zr)
                    gated_v[g, spot, :] = (
                        open_v[g, spot, :] * mixed_v[g, b, o].astype(jnp.float32)
                    ).astype(jnp.bfloat16)
                hand_over(g, o)

    for o in range(zs):
        for r in range(1, sp):
            if not (square and r == 3):
                arrived(ow_piece(source(r), o, c), pl_r.at[r, o])
        go(plane_second(o))
        for r in range(1, sp):
            if not (square and r == 3):
                go(plane_pair(r, o))

    unit(zs - 1, only=zs - 1)
    for o in range(zs - 1):
        unit(o)
        if o == 0 and held_back < groups:
            each_d(late_mix, lambda zz: late(zz, zz + 1))

    if square:
        for o in range(zs):
            arrived(ow_piece(source(3), o, c), pl_r.at[3, o])
            go(plane_pair(3, o))

    def gone(copies):
        for copy in copies:
            copy.wait_send()

    def line_gone(zz):
        for o in range(zs):
            for h in range(2):
                gone(ug_copies(zz, o, h))
            gone(ow_down(zz, o) + ow_rise(zz, o))
        if not inner(zz):
            gone([v_copy(zz, q) for q in range(sp) if v_useful(zz, q)])

    gone(tok_first() + tok_second())
    for o in range(zs):
        gone(plane_first(o) + ow_pair(o))
        for r in range(1, sp):
            if not (square and r == 3):
                gone(plane_pair(r, o))
    each_z(line_gone)

    per_part = groups // parts

    def gather_part(p):
        for s in range(sp):
            @pl.when(me != s)
            def _():
                for g in range(p * per_part, (p + 1) * per_part):
                    arrived(held_v.at[s, g], ga_r.at[g, s])
        squares = jnp.zeros((per, gd), jnp.float32)
        for s in range(sp):
            for i in range(per_part):
                g = p * per_part + i
                value = held_v[s, g].astype(jnp.float32)
                squares += value * value
                cols = slice(s * chans + g * gd, s * chans + (g + 1) * gd)
                normed_v[p, :, s * pk + i * gd:s * pk + (i + 1) * gd] = (
                    value * ogain_ref[:, cols]).astype(jnp.bfloat16)
        sums_v[...] = squares if p == 0 else sums_v[...] + squares

    def part_dot(p, cols):
        return jnp.dot(normed_v[p], outw_v[p, :, :, cols].reshape(sp * pk, ncol),
                       preferred_element_type=jnp.float32)

    def weights_here():
        for o in range(zs):
            arrived(ow_piece(me, o, 1 - c), ow_pr.at[o])
            for r in range(1, sp):
                arrived(ow_piece(source(r), o, 1 - c), pp_r.at[r, o])

    weights_here()
    if parts > 1:
        unit(zs - 1, 0, groups - 1, but=zs - 1)
        gather_part(0)

        @pl.loop(0, width // ncol)
        def _(t):
            cols = pl.ds(pl.multiple_of(t * ncol, LANES), ncol)
            part_v[:, cols] = part_dot(0, cols)

        unit(zs - 1, groups - 1, groups, but=zs - 1)
    else:
        unit(zs - 1, but=zs - 1)
    gather_part(parts - 1)
    scale = lax.rsqrt(jnp.sum(sums_v[...], axis=-1, keepdims=True) / (sp * chans) + norm_eps)

    @pl.loop(0, width // ncol)
    def _(t):
        cols = pl.ds(pl.multiple_of(t * ncol, LANES), ncol)
        last = part_dot(parts - 1, cols)
        if parts > 1:
            last += part_v[:, cols]
        out_ref[:, cols] = (last * scale).astype(jnp.bfloat16)

    for o in range(zs):
        gone(plane_second(o))
        if square:
            gone(plane_pair(3, o))

    def rest_gone(zz):
        @pl.loop(0, groups)
        def _(g):
            gone([ret_copy(zz, g, o) for o in range(zs) if with_mate(zz, o)])

    each_z(rest_gone, lambda zz: inner(zz) and mate(zz) is not None)

    def mix_gone(zz, cc):
        @pl.loop(0, groups)
        def _(g):
            for o in range(zs):
                if o == zz:
                    ways = ("dn", "up", "pair")
                elif inner(zz):
                    ways = ("dn" if o > zz else "up", "pair")
                else:
                    ways = ()
                for way in ways:
                    gone(mx_copies(zz, cc, g, o, way))

    each_d(mix_gone)
    for q in range(sp):
        @pl.when(me != q)
        def _():
            @pl.loop(0, groups)
            def _(g):
                gone([gated_copy(g, q)])


def body(tokens, up_weight, gate_weight, group_gain, mix_weight, mix_bias, out_gain, out_weight):
    per, width = tokens.shape[1:]
    groups, gd = group_gain.shape
    rows, block = mix_weight.shape[1:]
    sp, dps = lax.axis_size("sp"), lax.axis_size("dp")
    zs = dps // CORES
    total = sp * per
    parts = 1 if groups % 2 else 2
    bf, f32 = jnp.bfloat16, jnp.float32
    dma = pltpu.SemaphoreType.DMA
    hbm = pl.BlockSpec(memory_space=pltpu.HBM)
    vmem = pl.BlockSpec(memory_space=pltpu.VMEM)
    output = pl.pallas_call(
        functools.partial(fused_kernel, sp, zs),
        out_shape=pltpu.VMEM((per, width), bf),
        in_specs=[hbm, hbm, hbm, vmem, hbm, vmem, vmem, hbm],
        out_specs=vmem,
        scratch_shapes=[
            pltpu.VMEM((sp, per, width), bf),
            pltpu.VMEM((width, 2 * groups * gd), bf),
            pltpu.VMEM((groups, dps, rows, block), bf),
            pltpu.VMEM((parts, sp, groups * gd // parts, width), bf),
            pltpu.VMEM((groups, total, gd), f32),
            pltpu.VMEM((groups, total, gd), bf),
            pltpu.VMEM((groups, total, gd), bf),
            pltpu.VMEM((groups, block, gd), f32),
            pltpu.VMEM((groups, total // block, zs, CORES * rows, gd), bf),
            pltpu.VMEM((groups, total, gd), bf),
            pltpu.VMEM((sp, groups, per, gd), bf),
            pltpu.VMEM((parts, per, sp * groups * gd // parts), bf),
            pltpu.VMEM((per, gd), f32),
            pltpu.VMEM((per, width if parts > 1 else gd), f32),
            dma((3 + 2 * groups + parts,)),
        ] + [dma((zs, 2))] * 5 + [dma((zs,))] * 5 + [dma((sp, zs))] * 4
        + [dma((groups, zs, 2))] * 5 + [dma((sp, 2))] * 2 + [dma((sp,))] * 2
        + [dma((groups, zs))] * 2 + [dma((groups, sp))] * 2,
        compiler_params=pltpu.CompilerParams(collective_id=0, has_side_effects=True, vmem_limit_bytes=65_000_000),
    )(tokens.reshape(per, width), up_weight, gate_weight, group_gain[:, None, :], mix_weight, mix_bias,
      out_gain[None, :], out_weight)
    return output.reshape(tokens.shape)


def solution(mesh):
    return jax.shard_map(
        body,
        mesh=mesh,
        in_specs=(
            P("dp", "sp", None),
            P("dp", None),
            P("dp", None),
            P("sp", None),
            P("sp", "dp", None),
            P("sp", None),
            P(),
            P(None, "dp"),
        ),
        out_specs=P("dp", "sp", None),
        check_vma=False,
    )
```

profile of v0, /device:TPU:7, one launch (start us, length us, event | category | flops | bytes accessed | tf_op | source)
XLA Modules:
  0.0 115.7 jit_solution(5558440163809126711)
XLA Ops:
  0.0 114.7 %shard_map.82 = bf16[320,2048]{1,0:T(8,128)(2,1)S(1)} custom-call(bf16[320,2048]{1,0:T(8,128)(2,1)} %bitcast.5, bf16[256,2048]{1,0:T(8,128)(2,1)} %up_ref.1, bf16[256,2048]{1,0:T(8,128)(2,1)} %gate_ref.1, f32[4,1,128]{2,1,0:T(1,128)} %bitcast.7, bf16[4,160,1280]{2,1,0:T(8,128)(2,1)} %mix_ref.1, f32[4,1280]{1,0:T(4,128)} %bias_ref.1, f32[1,2048]{1,0:T(1,128)} %bitcast.6, ...), custom_call_target="tpu_custom_call" | custom-call | tf_op jit(solution)/shard_map/pallas_call | solution.py:676
  114.7 1.1 copy.10
where the time goes:
time: 116 us
  Pallas kernels  115 us (99%)
    pallas_call x1, Pallas kernels, body(): pl.pallas_call(functools.partial(fused_kernel, sp, zs), out_shape=pltpu.V...  115 us

commit v1 on v0

--- a/solution.py
+++ b/solution.py
@@ -22,10 +22,8 @@
     tok_ref, up_ref, gate_ref, gain_ref, mix_ref, bias_ref, ogain_ref, outw_ref, out_ref,
     tok_v, ug_v, mix_v, outw_v, open_v, norm_v, other_v, bias_v, mixed_v, gated_v, held_v,
     normed_v, sums_v, part_v,
-    load_sem,
-    ug_line, ug_up, ug_dn, ug_ps, ug_pr,
-    ow_line, ow_up, ow_dn, ow_ps, ow_pr, pl_s, pl_r, pp_s, pp_r,
-    mx_line, mx_up, mx_dn, mx_ps, mx_pr,
+    load_sem, ug_line, ug_send, ug_pr, ow_line, ow_send, ow_pr, ow_own,
+    pl_s, pl_r, p2_s, p2_r, pp_s, pp_r, mx_line, mx_pr, mx_up, mx_dn, mx_ps,
     tok_s, tok_r, v_s, v_r, ret_s, ret_r, ga_s, ga_r,
 ):
     me = lax.axis_index("sp")
@@ -35,9 +33,10 @@
     per, width = out_ref.shape
     gd = gain_ref.shape[2]
     chans = groups * gd
-    depth, ncol = up_ref.shape[0], outw_ref.shape[1]
+    depth, ncol = up_ref.shape[0], outw_ref.shape[3]
     total = sp * per
     blocks = total // block
+    per_part = groups // outw_v.shape[0]
     parts, _, pk, _ = outw_v.shape
     zr = CORES * rows
     half, dhalf = per // 2, depth // 2
@@ -74,6 +73,9 @@
         return pltpu.make_async_remote_copy(
             src_ref=src, dst_ref=dst, send_sem=send, recv_sem=recv,
             device_id=device, device_id_type=MESH)
+
+    def sent(ref, sem):
+        remote(ref, ref, sem, sem, partner).wait_send()
 
     def arrived(ref, sem):
         remote(ref, ref, sem, sem, partner).wait_recv()
@@ -97,17 +99,19 @@
             loads["ug"].append(pltpu.make_async_copy(
                 ref.at[:, cols],
                 ug_v.at[pl.ds(dp * depth, depth), pl.ds(spot * gd, gd)],
-                load_sem.at[3 + spot]))
+                load_sem.at[3]))
     loads["tok"].append(pltpu.make_async_copy(tok_ref, tok_v.at[me], load_sem.at[0]))
+    own_cols = pl.ds(pl.multiple_of(dp * ncol, LANES), ncol)
     for p in range(parts):
         loads["ow"].append(pltpu.make_async_copy(
-            outw_ref.at[pl.ds(me * chans + p * pk, pk), :],
-            outw_v.at[p, me, :, pl.ds(pl.multiple_of(dp * ncol, LANES), ncol)],
-            load_sem.at[3 + 2 * groups + p]))
+            outw_ref.at[:, p], outw_v.at[p, :, :, own_cols], load_sem.at[1]))
     loads["mx"].append(pltpu.make_async_copy(mix_ref, mix_v.at[:, dp], load_sem.at[2]))
     for kind in ("ug", "tok", "ow", "mx"):
         for load in loads[kind]:
             load.start()
+
+    def loaded(ref, sem):
+        pltpu.make_async_copy(ref, ref, sem).wait()
 
     barrier = pltpu.get_barrier_semaphore()
 
@@ -145,27 +149,34 @@
     def ug_copies(zz, o, h):
         src, out = ug_piece(o, c, h), []
         if o >= zz and zz > 0:
-            out.append(remote(src, src, ug_dn.at[o, h], ug_line.at[o, h], at_line(zz - 1)))
+            out.append(remote(src, src, ug_send.at[1], ug_line.at[o, h], at_line(zz - 1)))
         if o <= zz and zz < zs - 1:
-            out.append(remote(src, src, ug_up.at[o, h], ug_line.at[o, h], at_line(zz + 1)))
-        out.append(remote(src, src, ug_ps.at[o, h], ug_pr.at[o, h], partner))
+            out.append(remote(src, src, ug_send.at[0], ug_line.at[o, h], at_line(zz + 1)))
+        out.append(remote(src, src, ug_send.at[2], ug_pr.at[0], partner))
         return out
 
     def ow_down(zz, o):
         src = ow_piece(me, o, c)
         if o >= zz and zz > 0:
-            return [remote(src, src, ow_dn.at[o], ow_line.at[o], at_line(zz - 1))]
+            return [remote(src, src, ow_send.at[1], ow_line.at[o], at_line(zz - 1))]
         return []
 
     def ow_rise(zz, o):
         src = ow_piece(me, o, c)
         if o <= zz and zz < zs - 1:
-            return [remote(src, src, ow_up.at[o], ow_line.at[o], at_line(zz + 1))]
+            return [remote(src, src, ow_send.at[0], ow_line.at[o], at_line(zz + 1))]
         return []
 
     def ow_pair(o):
         src = ow_piece(me, o, c)
-        return [remote(src, src, ow_ps.at[o], ow_pr.at[o], partner)]
+        return [remote(src, src, ow_send.at[2], ow_pr.at[0], partner)]
+
+    def ow_own_pair():
+        src = outw_v.at[:, :, :, own_cols]
+        return [remote(src, src, ow_own.at[0], ow_own.at[1], partner)]
+
+    def ow_bytes(n):
+        return outw_v.at[:, 0, :, pl.ds(0, n * ncol)]
 
     def mx_copies(zz, cc, g, o, way):
         out = []
@@ -173,11 +184,11 @@
         for i, piece in enumerate(cuts(d)):
             src = mx_piece(g, d, piece)
             if way == "dn" and o >= zz and inner(zz - 1):
-                out.append(remote(src, src, mx_dn.at[g, o, i], mx_line.at[g, o, i], at_line(zz - 1)))
+                out.append(remote(src, src, mx_dn.at[o, i], mx_line.at[g, o, i], at_line(zz - 1)))
             if way == "up" and o <= zz and inner(zz + 1):
-                out.append(remote(src, src, mx_up.at[g, o, i], mx_line.at[g, o, i], at_line(zz + 1)))
+                out.append(remote(src, src, mx_up.at[o, i], mx_line.at[g, o, i], at_line(zz + 1)))
             if way == "pair" and (inner(zz) or o == zz):
-                out.append(remote(src, src, mx_ps.at[g, o, i], mx_pr.at[g, o, i], partner))
+                out.append(remote(src, src, mx_ps.at[o, i], mx_pr.at[g, o, i], partner))
         return out
 
     def go(copies):
@@ -202,8 +213,7 @@
     def own_out(zz, way):
         go(ow_down(zz, zz) if way == "dn" else ow_rise(zz, zz))
 
-    for load in loads["ug"]:
-        load.wait()
+    loaded(ug_v.at[pl.ds(dp * depth, depth), :], load_sem.at[3])
 
     def first_weights(zz):
         for h in range(2):
@@ -217,7 +227,7 @@
         return tok_v.at[s, pl.ds(h * half, half), :]
 
     def tok_copy(s, r, h, r_there):
-        return remote(tok_half(s, h), tok_half(s, h), tok_s.at[r_there, h], tok_r.at[r_there, h], peer(r))
+        return remote(tok_half(s, h), tok_half(s, h), tok_s.at[0], tok_r.at[r_there, h], peer(r))
 
     def tok_first():
         if square:
@@ -230,11 +240,11 @@
         return []
 
     go(tok_first())
-    for load in loads["ow"] + loads["mx"]:
-        load.wait()
+    loaded(outw_v.at[:, :, :, own_cols], load_sem.at[1])
+    loads["mx"][0].wait()
+    go(ow_own_pair())
 
     def first_rest(zz):
-        go(ow_pair(zz))
         for way in ("dn", "up"):
             there, left = ug_left(zz, way, 0)
             if there and left == 0:
@@ -274,21 +284,32 @@
             if there and left == 0 and before > 0:
                 own_mix(zz, way, 1, groups)
 
+    def others(zz):
+        return [o for k in range(1, zs) for o in (zz + k, zz - k) if 0 <= o < zs]
+
     def plane_first(o):
         src = ow_piece(me, o, c)
         reach = (1, 2) if square else range(1, sp)
-        return [remote(src, src, pl_s.at[r, o], pl_r.at[r, o], peer(r)) for r in reach]
-
-    def plane_second(o):
+        return [remote(src, src, pl_s.at[r], pl_r.at[r, o], peer(r)) for r in reach]
+
+    def second_part(s, o, p):
+        cols = pl.ds(pl.multiple_of((o * CORES + c) * ncol, LANES), ncol)
+        return outw_v.at[p, s, :, cols]
+
+    def plane_second(zz, o):
         if not square:
             return []
-        via, to = (1, 2) if o < zs // 2 else (2, 1)
-        src = ow_piece(source(via), o, c)
-        return [remote(src, src, pl_s.at[3, o], pl_r.at[3, o], peer(to))]
+        units = [(x, p) for x in others(zz) for p in range(parts)]
+        out = []
+        for p in range(parts):
+            via, to = (1, 2) if units.index((o, p)) < len(units) // 2 else (2, 1)
+            src = second_part(source(via), o, p)
+            out.append(remote(src, src, p2_s.at[0], p2_r.at[o, p], peer(to)))
+        return out
 
     def plane_pair(r, o):
         src = ow_piece(source(r), o, c)
-        return [remote(src, src, pp_s.at[r, o], pp_r.at[r, o], partner)]
+        return [remote(src, src, pp_s.at[r], pp_r.at[r], partner)]
 
     each_z(lambda zz: take_ug(zz, 1))
     if square:
@@ -302,24 +323,17 @@
         if inner(zz) and not square:
             for k in range(1, zs):
                 take_out(zz, k)
-            for o in range(zs):
+            for o in others(zz):
                 go(plane_first(o))
-        if not inner(zz):
-            go(plane_first(zz))
 
     each_z(more_weights)
 
-    def weights_in(zz):
-        for o in range(zs):
-            for h in range(2):
-                arrived(ug_piece(o, 1 - c, h), ug_pr.at[o, h])
-
-    weights_in(None)
+    arrived(ug_v.at[pl.ds(0, zs * depth), :], ug_pr.at[0])
 
     def v_copy(zz, q):
         spot = pl.ds(pl.multiple_of(q * per, 16), per)
         return remote(norm_v.at[:, spot, :], other_v.at[:, spot, :],
-                      v_s.at[q], v_r.at[q], at_line(mate(zz)))
+                      v_s.at[0], v_r.at[q], at_line(mate(zz)))
 
     def starts(q):
         return (q * per) % block
@@ -356,8 +370,6 @@
             for o in (zz + k, zz - k):
                 if 0 <= o < zs:
                     go(plane_first(o))
-            if inner(zz) and k == 1:
-                go(plane_first(zz))
 
     if square:
         for r in range(sp):
@@ -435,11 +447,11 @@
 
     def gated_copy(g, q):
         return remote(gated_v.at[g, pl.ds(q * per, per), :], held_v.at[me, g],
-                      ga_s.at[g, q], ga_r.at[g, me], {"sp": q})
+                      ga_s.at[0], ga_r.at[g // per_part, me], {"sp": q})
 
     def ret_copy(zz, g, o):
         spot = mixed_v.at[g, :, o]
-        return remote(spot, spot, ret_s.at[g, o], ret_r.at[g, o], at_line(mate(zz)))
+        return remote(spot, spot, ret_s.at[0], ret_r.at[g, o], at_line(mate(zz)))
 
     def hand_over(g, o):
         for q in range(sp):
@@ -534,14 +546,23 @@
                     ).astype(jnp.bfloat16)
                 hand_over(g, o)
 
-    for o in range(zs):
-        for r in range(1, sp):
-            if not (square and r == 3):
-                arrived(ow_piece(source(r), o, c), pl_r.at[r, o])
-        go(plane_second(o))
-        for r in range(1, sp):
-            if not (square and r == 3):
-                go(plane_pair(r, o))
+    def plane_round(zz):
+        for o in others(zz):
+            for r in range(1, sp):
+                if not (square and r == 3):
+                    arrived(ow_piece(source(r), o, c), pl_r.at[r, o])
+            go(plane_second(zz, o))
+            for r in range(1, sp):
+                if not (square and r == 3):
+                    go(plane_pair(r, o))
+
+    def plane_end(zz):
+        for o in others(zz):
+            for p in range(parts):
+                arrived(second_part(source(3), o, p), p2_r.at[o, p])
+            go(plane_pair(3, o))
+
+    each_z(plane_round)
 
     unit(zs - 1, only=zs - 1)
     for o in range(zs - 1):
@@ -550,38 +571,13 @@
             each_d(late_mix, lambda zz: late(zz, zz + 1))
 
     if square:
-        for o in range(zs):
-            arrived(ow_piece(source(3), o, c), pl_r.at[3, o])
-            go(plane_pair(3, o))
-
-    def gone(copies):
-        for copy in copies:
-            copy.wait_send()
-
-    def line_gone(zz):
-        for o in range(zs):
-            for h in range(2):
-                gone(ug_copies(zz, o, h))
-            gone(ow_down(zz, o) + ow_rise(zz, o))
-        if not inner(zz):
-            gone([v_copy(zz, q) for q in range(sp) if v_useful(zz, q)])
-
-    gone(tok_first() + tok_second())
-    for o in range(zs):
-        gone(plane_first(o) + ow_pair(o))
-        for r in range(1, sp):
-            if not (square and r == 3):
-                gone(plane_pair(r, o))
-    each_z(line_gone)
-
-    per_part = groups // parts
+        each_z(plane_end)
 
     def gather_part(p):
         for s in range(sp):
             @pl.when(me != s)
             def _():
-                for g in range(p * per_part, (p + 1) * per_part):
-                    arrived(held_v.at[s, g], ga_r.at[g, s])
+                arrived(held_v.at[s, pl.ds(p * per_part, per_part)], ga_r.at[p, s])
         squares = jnp.zeros((per, gd), jnp.float32)
         for s in range(sp):
             for i in range(per_part):
@@ -598,10 +594,10 @@
                        preferred_element_type=jnp.float32)
 
     def weights_here():
-        for o in range(zs):
-            arrived(ow_piece(me, o, 1 - c), ow_pr.at[o])
-            for r in range(1, sp):
-                arrived(ow_piece(source(r), o, 1 - c), pp_r.at[r, o])
+        arrived(outw_v.at[:, :, :, own_cols], ow_own.at[1])
+        arrived(ow_bytes(zs - 1), ow_pr.at[0])
+        for r in range(1, sp):
+            arrived(ow_bytes(zs - 1), pp_r.at[r])
 
     weights_here()
     if parts > 1:
@@ -627,38 +623,46 @@
             last += part_v[:, cols]
         out_ref[:, cols] = (last * scale).astype(jnp.bfloat16)
 
-    for o in range(zs):
-        gone(plane_second(o))
-        if square:
-            gone(plane_pair(3, o))
-
-    def rest_gone(zz):
-        @pl.loop(0, groups)
-        def _(g):
-            gone([ret_copy(zz, g, o) for o in range(zs) if with_mate(zz, o)])
-
-    each_z(rest_gone, lambda zz: inner(zz) and mate(zz) is not None)
-
-    def mix_gone(zz, cc):
-        @pl.loop(0, groups)
-        def _(g):
-            for o in range(zs):
-                if o == zz:
-                    ways = ("dn", "up", "pair")
-                elif inner(zz):
-                    ways = ("dn" if o > zz else "up", "pair")
-                else:
-                    ways = ()
-                for way in ways:
-                    gone(mx_copies(zz, cc, g, o, way))
-
-    each_d(mix_gone)
-    for q in range(sp):
-        @pl.when(me != q)
-        def _():
-            @pl.loop(0, groups)
-            def _(g):
-                gone([gated_copy(g, q)])
+    sent(tok_v.at[pl.ds(0, sp - 1)], tok_s.at[0])
+    sent(outw_v.at[:, :, :, own_cols], ow_own.at[0])
+    for r in range(1, sp):
+        if not (square and r == 3):
+            sent(ow_bytes(zs - 1), pl_s.at[r])
+        sent(ow_bytes(zs - 1), pp_s.at[r])
+    if square:
+        sent(ow_bytes(zs - 1), p2_s.at[0])
+    sent(ow_bytes(zs - 1), ow_send.at[2])
+    sent(ug_v.at[pl.ds(0, zs * depth), :], ug_send.at[2])
+    sent(held_v.at[pl.ds(0, sp - 1)], ga_s.at[0])
+
+    def line_sent(zz):
+        for n, way in ((zz + 1 if zz < zs - 1 else 0, 0), (zs - zz if zz > 0 else 0, 1)):
+            if n:
+                sent(ug_v.at[pl.ds(0, n * depth), :], ug_send.at[way])
+                sent(ow_bytes(n), ow_send.at[way])
+        if not inner(zz):
+            n = sum(v_useful(zz, q) for q in range(sp))
+            sent(norm_v.at[:, pl.ds(0, n * per), :], v_s.at[0])
+        elif mate(zz) is not None:
+            n = sum(with_mate(zz, o) for o in range(zs))
+            sent(mixed_v.at[:, :, pl.ds(0, n)], ret_s.at[0])
+
+    each_z(line_sent)
+
+    def mix_sent(zz, cc):
+        for o in range(zs):
+            d = o * CORES + cc
+            for i, (r0, rn, cols) in enumerate(cuts(d)):
+                spot = mix_v.at[:, d, pl.ds(r0, rn), pl.ds(0, cols)]
+                if not (inner(zz) or o == zz):
+                    continue
+                if o >= zz and inner(zz - 1):
+                    sent(spot, mx_dn.at[o, i])
+                if o <= zz and inner(zz + 1):
+                    sent(spot, mx_up.at[o, i])
+                sent(spot, mx_ps.at[o, i])
+
+    each_d(mix_sent)
 
 
 def body(tokens, up_weight, gate_weight, group_gain, mix_weight, mix_bias, out_gain, out_weight):
@@ -693,13 +697,17 @@
             pltpu.VMEM((parts, per, sp * groups * gd // parts), bf),
             pltpu.VMEM((per, gd), f32),
             pltpu.VMEM((per, width if parts > 1 else gd), f32),
-            dma((3 + 2 * groups + parts,)),
-        ] + [dma((zs, 2))] * 5 + [dma((zs,))] * 5 + [dma((sp, zs))] * 4
-        + [dma((groups, zs, 2))] * 5 + [dma((sp, 2))] * 2 + [dma((sp,))] * 2
-        + [dma((groups, zs))] * 2 + [dma((groups, sp))] * 2,
+            dma((4,)),
+            dma((zs, 2)), dma((3,)), dma((1,)),
+            dma((zs,)), dma((3,)), dma((1,)), dma((2,)),
+            dma((sp,)), dma((sp, zs)), dma((1,)), dma((zs, parts)), dma((sp,)), dma((sp,)),
+            dma((groups, zs, 2)), dma((groups, zs, 2)), dma((zs, 2)), dma((zs, 2)), dma((zs, 2)),
+            dma((1,)), dma((sp, 2)), dma((1,)), dma((sp,)),
+            dma((1,)), dma((groups, zs)), dma((1,)), dma((parts, sp)),
+        ],
         compiler_params=pltpu.CompilerParams(collective_id=0, has_side_effects=True, vmem_limit_bytes=65_000_000),
     )(tokens.reshape(per, width), up_weight, gate_weight, group_gain[:, None, :], mix_weight, mix_bias,
-      out_gain[None, :], out_weight)
+      out_gain[None, :], out_weight.reshape(sp, parts, groups * gd // parts, -1))
     return output.reshape(tokens.shape)
 
 

time: 116 us -> 110 us (0.948); the launches traced: 116 us -> 108 us
  Pallas kernels: 115 us -> 107 us
    pallas_call x1, Pallas kernels: 115 us -> 107 us  [body(): pl.pallas_call(functools.partial(fused_kernel, sp, zs), out_shape=pltpu.V...]
where the time goes in v1:
time: 110 us; the launch traced here: 108 us
  Pallas kernels  107 us (97%)
    pallas_call x1, Pallas kernels, body(): pl.pallas_call(functools.partial(fused_kernel, sp, zs), out_shape=pltpu.V...  107 us

profile of v1, /device:TPU:7, one launch (start us, length us, event | category | flops | bytes accessed | tf_op | source)
XLA Modules:
  0.0 108.4 jit_solution(2884788239745145870)
XLA Ops:
  0.0 107.4 %shard_map.82 = bf16[320,2048]{1,0:T(8,128)(2,1)S(1)} custom-call(bf16[320,2048]{1,0:T(8,128)(2,1)} %bitcast.6, bf16[256,2048]{1,0:T(8,128)(2,1)} %up_ref.1, bf16[256,2048]{1,0:T(8,128)(2,1)} %gate_ref.1, f32[4,1,128]{2,1,0:T(1,128)} %bitcast.9, bf16[4,160,1280]{2,1,0:T(8,128)(2,1)} %mix_ref.1, f32[4,1280]{1,0:T(4,128)} %bias_ref.1, f32[1,2048]{1,0:T(1,128)} %bitcast.8, ...), custom_call_target="tpu_custom_call" | custom-call | tf_op jit(solution)/shard_map/pallas_call | solution.py:680
  107.4 1.1 copy.10

commit v2 on v1

--- a/solution.py
+++ b/solution.py
@@ -21,10 +21,10 @@
     sp, zs,
     tok_ref, up_ref, gate_ref, gain_ref, mix_ref, bias_ref, ogain_ref, outw_ref, out_ref,
     tok_v, ug_v, mix_v, outw_v, open_v, norm_v, other_v, bias_v, mixed_v, gated_v, held_v,
-    normed_v, sums_v, part_v,
+    normed_v, sums_v, part_v, far_v, far_m,
     load_sem, ug_line, ug_send, ug_pr, ow_line, ow_send, ow_pr, ow_own,
     pl_s, pl_r, p2_s, p2_r, pp_s, pp_r, mx_line, mx_pr, mx_up, mx_dn, mx_ps,
-    tok_s, tok_r, v_s, v_r, ret_s, ret_r, ga_s, ga_r,
+    tok_s, tok_r, v_s, v_r, ret_s, ret_r, ga_s, ga_r, fv_s, fv_r, fm_s, fm_r,
 ):
     me = lax.axis_index("sp")
     dp = lax.axis_index("dp")
@@ -36,11 +36,14 @@
     depth, ncol = up_ref.shape[0], outw_ref.shape[3]
     total = sp * per
     blocks = total // block
-    per_part = groups // outw_v.shape[0]
     parts, _, pk, _ = outw_v.shape
+    halves = 1 if parts % 2 else 2
+    hp = parts // halves
     zr = CORES * rows
     half, dhalf = per // 2, depth // 2
     square = sp == 4
+    far = zs == 4 and groups > 2
+    below, above, last_g = zs // 2 - 1, zs // 2, groups - 1
 
     partner = {"dp": z * CORES + (1 - c)}
 
@@ -142,6 +145,10 @@
             at = top
         return out
 
+    def mx_bytes(d):
+        size = sum(rn * cols for _, rn, cols in cuts(d))
+        return open_v.at[0, pl.ds(0, size // gd // 2), :]
+
     def mx_piece(g, d, piece):
         r0, rn, cols = piece
         return mix_v.at[g, d, pl.ds(r0, rn), pl.ds(0, cols)]
@@ -184,11 +191,11 @@
         for i, piece in enumerate(cuts(d)):
             src = mx_piece(g, d, piece)
             if way == "dn" and o >= zz and inner(zz - 1):
-                out.append(remote(src, src, mx_dn.at[o, i], mx_line.at[g, o, i], at_line(zz - 1)))
+                out.append(remote(src, src, mx_dn.at[o, i], mx_line.at[g, o], at_line(zz - 1)))
             if way == "up" and o <= zz and inner(zz + 1):
-                out.append(remote(src, src, mx_up.at[o, i], mx_line.at[g, o, i], at_line(zz + 1)))
+                out.append(remote(src, src, mx_up.at[o, i], mx_line.at[g, o], at_line(zz + 1)))
             if way == "pair" and (inner(zz) or o == zz):
-                out.append(remote(src, src, mx_ps.at[o, i], mx_pr.at[g, o, i], partner))
+                out.append(remote(src, src, mx_ps.at[o, i], mx_pr.at[g, o], partner))
         return out
 
     def go(copies):
@@ -196,6 +203,9 @@
             copy.start()
 
     def own_mix(zz, way, low=0, high=groups):
+        if far and zz == above and way == "dn":
+            high = min(high, last_g)
+
         for cc in range(CORES):
             @pl.when(c == cc)
             def _():
@@ -294,14 +304,14 @@
 
     def second_part(s, o, p):
         cols = pl.ds(pl.multiple_of((o * CORES + c) * ncol, LANES), ncol)
-        return outw_v.at[p, s, :, cols]
+        return outw_v.at[pl.ds(p * hp, hp), s, :, cols]
 
     def plane_second(zz, o):
         if not square:
             return []
-        units = [(x, p) for x in others(zz) for p in range(parts)]
+        units = [(x, p) for x in others(zz) for p in range(halves)]
         out = []
-        for p in range(parts):
+        for p in range(halves):
             via, to = (1, 2) if units.index((o, p)) < len(units) // 2 else (2, 1)
             src = second_part(source(via), o, p)
             out.append(remote(src, src, p2_s.at[0], p2_r.at[o, p], peer(to)))
@@ -330,10 +340,18 @@
 
     arrived(ug_v.at[pl.ds(0, zs * depth), :], ug_pr.at[0])
 
-    def v_copy(zz, q):
+    def split(zz):
+        return far and zz == below - 1
+
+    def v_copies(zz, q):
         spot = pl.ds(pl.multiple_of(q * per, 16), per)
-        return remote(norm_v.at[:, spot, :], other_v.at[:, spot, :],
-                      v_s.at[0], v_r.at[q], at_line(mate(zz)))
+        ranges = ((last_g, 1), (0, last_g)) if split(zz) else ((0, groups),)
+        out = []
+        for i, (g0, gn) in enumerate(ranges):
+            which = len(ranges) - 1 - i
+            src, dst = (ref.at[pl.ds(g0, gn), spot, :] for ref in (norm_v, other_v))
+            out.append(remote(src, dst, v_s.at[which], v_r.at[which, q], at_line(mate(zz))))
+        return out
 
     def starts(q):
         return (q * per) % block
@@ -344,7 +362,10 @@
     def send_v(zz, s):
         for q in range(sp):
             if v_useful(zz, q):
-                pl.when(s == q)(lambda q=q: v_copy(zz, q).start())
+                pl.when(s == q)(lambda q=q: go(v_copies(zz, q)))
+
+    def far_send(i, ref):
+        return remote(ref.at[last_g], far_v.at[i], fv_s.at[i], fv_r.at[i], at_line(above))
 
     def project(s):
         spot = pl.ds(pl.multiple_of(s * per, 16), per)
@@ -372,11 +393,17 @@
                     go(plane_first(o))
 
     if square:
+        def in_order(i):
+            place = jnp.where(me == sp - 1, 1 - i, i) if i < 2 else i
+            return jnp.where((z == 0) | (z == zs - 1), source(place), i)
+
         for r in range(sp):
-            for h in range(2 if r else 0):
-                if r != 1 + h:
-                    arrived(tok_half(source(r), h), tok_r.at[r, h])
-            project(source(r))
+            turn = in_order(r)
+            for h in range(2):
+                @pl.when((turn > 0) & (turn != 1 + h))
+                def _():
+                    arrived(tok_half(source(turn), h), tok_r.at[turn, h])
+            project(source(turn))
 
             def events(zz, r=r):
                 first = r + 1 if inner(zz) else r
@@ -396,14 +423,11 @@
 
         each_z(lambda zz: out_events(zz, range(1, zs)), lambda zz: not inner(zz))
 
-    if held_back < groups:
-        each_z(lambda zz: own_mix(zz, "dn", held_back, groups), lambda zz: zz == zs - 1)
-
-    def take_mix(zz, cc, g, o):
+    def take_mix(zz, cc, g, o, onward=True):
         d = o * CORES + cc
-        for i, piece in enumerate(cuts(d)):
-            arrived(mx_piece(g, d, piece), mx_line.at[g, o, i])
-        go(mx_copies(zz, cc, g, o, "dn" if o > zz else "up"))
+        arrived(mx_bytes(d), mx_line.at[g, o])
+        if onward:
+            go(mx_copies(zz, cc, g, o, "dn" if o > zz else "up"))
         go(mx_copies(zz, cc, g, o, "pair"))
 
     def passed_on(zz, o):
@@ -422,9 +446,11 @@
     def late_mix(zz, cc):
         @pl.loop(held_back, groups)
         def _(g):
-            take_mix(zz, cc, g, zz + 1)
+            take_mix(zz, cc, g, zz + 1, not far)
 
     each_d(near_mix, inner)
+    if far:
+        each_z(lambda zz: far_send(0, norm_v).start(), lambda zz: zz == below)
 
     def ready_at(q):
         if block % per:
@@ -437,7 +463,7 @@
     def first_need(zz, q):
         if not v_useful(mate(zz), q):
             return None
-        return next(o for o in range(zs) if o != mate(zz) and (block % per or starts(q) < needs(o)))
+        return next(o for o in range(zs) if o != mate(zz) and (block % per or starts(q) < (o + 1) * zr))
 
     def with_mate(zz, o):
         return inner(zz) and mate(zz) is not None and mate(zz) != o
@@ -447,7 +473,7 @@
 
     def gated_copy(g, q):
         return remote(gated_v.at[g, pl.ds(q * per, per), :], held_v.at[me, g],
-                      ga_s.at[0], ga_r.at[g // per_part, me], {"sp": q})
+                      ga_s.at[0], ga_r.at[g, me], {"sp": q})
 
     def ret_copy(zz, g, o):
         spot = mixed_v.at[g, :, o]
@@ -467,41 +493,46 @@
     def one_of(zs_in):
         return functools.reduce(jnp.logical_or, [z == zz for zz in zs_in])
 
-    def clear_unsent(zz):
-        for q in range(sp):
-            if not v_useful(mate(zz), q):
-                high = max(needs(o) for o in range(zs) if o != mate(zz)) - starts(q)
-                if high > 0:
-                    other_v[:, q * per:q * per + high, :] = jnp.zeros(
-                        (groups, high, gd), jnp.bfloat16)
-
-    each_z(clear_unsent, lambda zz: inner(zz) and mate(zz) is not None)
-
-    def unit(o, low=0, high=groups, only=None, but=None):
+    def unit(o, low=0, high=groups, only=None, but=()):
         lo = o * zr
         base, top = lo // LANES * LANES, needs(o)
 
         def wait_v(zz):
+            apart = split(mate(zz))
             for q in range(sp):
                 if first_need(zz, q) == o:
-                    arrived(other_v.at[:, pl.ds(q * per, per), :], v_r.at[q])
+                    rows_of = pl.ds(q * per, per)
+                    main = pl.ds(0, last_g if apart else groups)
+                    arrived(other_v.at[main, rows_of, :], v_r.at[0, q])
+                    if apart and o < above:
+                        arrived(other_v.at[pl.ds(last_g, 1), rows_of, :], v_r.at[1, q])
 
         if low == 0:
-            each_z(wait_v, lambda zz: with_mate(zz, o))
+            each_z(wait_v, lambda zz: with_mate(zz, o) and zz not in but and only in (None, zz))
 
         def mix(members, paired):
+            def rows_from_line(zz, cc):
+                @pl.loop(low, high)
+                def _(g):
+                    take_mix(zz, cc, g, o)
+
+            each_d(rows_from_line, lambda zz: zz in members and o != zz and not passed_on(zz, o))
+
             @pl.loop(low, high)
             def _(g):
                 def rows_in(zz, cc):
-                    if o != zz and not passed_on(zz, o):
-                        take_mix(zz, cc, g, o)
-                    d = o * CORES + 1 - cc
-                    for i, piece in enumerate(cuts(d)):
-                        arrived(mx_piece(g, d, piece), mx_pr.at[g, o, i])
-
-                def values(at, end):
+                    if not (far and zz == above and o == zs - 1 and low == last_g):
+                        arrived(mx_bytes(o * CORES + 1 - cc), mx_pr.at[g, o])
+
+                def values(at, end, spare=0):
                     own = norm_v[g, at:end, :]
-                    return jnp.concatenate([own, other_v[g, at:end, :]], axis=1) if paired else own
+                    if not paired:
+                        return own
+                    other = other_v[g, at:end - spare, :]
+                    if spare:
+                        zeros = jnp.zeros((spare, gd), jnp.bfloat16)
+                        other = jnp.concatenate([other, zeros], axis=0)
+                    return jnp.concatenate([own, other], axis=1)
 
                 each_d(rows_in, lambda zz: zz in members)
                 corner = mix_v[g, o * CORES:(o + 1) * CORES, :, base:top].reshape(zr, top - base)
@@ -511,7 +542,7 @@
                 bias = bias_v[g, lo:lo + zr, :]
                 for b in range(blocks):
                     at = b * block
-                    mixed = jnp.dot(corner, values(at + base, at + top),
+                    mixed = jnp.dot(corner, values(at + base, at + top, top - lo - zr),
                                     preferred_element_type=jnp.float32)
                     if base > 0:
                         left = mix_v[g, o * CORES:(o + 1) * CORES, :, :base].reshape(zr, base)
@@ -527,14 +558,18 @@
                 hand_over(g, o)
 
         for paired, test in ((True, with_mate), (False, alone)):
-            members = [zz for zz in range(zs) if test(zz, o) and zz != but and only in (None, zz)]
+            members = [zz for zz in range(zs) if test(zz, o) and zz not in but and only in (None, zz)]
             if members:
                 pl.when(one_of(members))(functools.partial(mix, members, paired))
 
         if only is not None:
             return
 
-        @pl.when(one_of([zz for zz in (0, zs - 1) if zz != o]))
+        waiting = [zz for zz in (0, zs - 1) if zz != o and zz not in but]
+        if not waiting:
+            return
+
+        @pl.when(one_of(waiting))
         def _():
             @pl.loop(low, high)
             def _(g):
@@ -547,7 +582,9 @@
                 hand_over(g, o)
 
     def plane_round(zz):
-        for o in others(zz):
+        for n, o in enumerate(others(zz)):
+            if n == 1 and zz == zs - 1 and held_back < groups:
+                own_mix(zz, "dn", held_back, groups)
             for r in range(1, sp):
                 if not (square and r == 3):
                     arrived(ow_piece(source(r), o, c), pl_r.at[r, o])
@@ -558,36 +595,107 @@
 
     def plane_end(zz):
         for o in others(zz):
-            for p in range(parts):
+            for p in range(halves):
                 arrived(second_part(source(3), o, p), p2_r.at[o, p])
             go(plane_pair(3, o))
 
+    def far_forward(zz):
+        for q in range(sp):
+            if first_need(zz, q) >= above:
+                arrived(other_v.at[pl.ds(last_g, 1), pl.ds(q * per, per), :], v_r.at[1, q])
+        far_send(1, other_v).start()
+
+    def far_unit(i):
+        o = above + i
+        lo, top = o * zr, needs(o)
+        base = lo // LANES * LANES
+        rows_of = slice(o * CORES, (o + 1) * CORES)
+        corner = mix_v[last_g, rows_of, :, base:top].reshape(zr, top - base)
+        keep = lax.broadcasted_iota(jnp.int32, corner.shape, 0) + (lo - base) >= (
+            lax.broadcasted_iota(jnp.int32, corner.shape, 1))
+        corner = jnp.where(keep, corner.astype(jnp.float32), 0.0).astype(jnp.bfloat16)
+        left = mix_v[last_g, rows_of, :, :base].reshape(zr, base)
+        bias = bias_v[last_g, lo:lo + zr, :]
+
+        def values(at, end):
+            return jnp.concatenate([far_v[0, at:end, :], far_v[1, at:end, :]], axis=1)
+
+        for b in range(blocks):
+            at = b * block
+            mixed = jnp.dot(left, values(at, at + base), preferred_element_type=jnp.float32)
+            mixed += jnp.dot(corner, values(at + base, at + top), preferred_element_type=jnp.float32)
+            for n in range(2):
+                far_m[n, i, b] = (mixed[:, n * gd:(n + 1) * gd] + bias).astype(jnp.bfloat16)
+
+    def far_back(i):
+        spot = far_m.at[:, i]
+        return remote(spot, spot, fm_s.at[i], fm_r.at[i], at_line(below))
+
+    def far_above(zz):
+        for i in range(2):
+            arrived(far_v.at[i], fv_r.at[i])
+        for cc in range(CORES):
+            @pl.when(c == cc)
+            def _():
+                arrived(mx_bytes((zs - 1) * CORES + 1 - cc), mx_pr.at[last_g, zs - 1])
+        for i in range(2):
+            far_unit(i)
+            far_back(i).start()
+
+    def far_ret(i):
+        return remote(far_m.at[1, i], mixed_v.at[last_g, :, above + i],
+                      ret_s.at[0], ret_r.at[last_g, above + i], at_line(below - 1))
+
+    def far_below(zz):
+        for i in range(2):
+            o = above + i
+            if zz == below:
+                arrived(far_m.at[:, i], fm_r.at[i])
+                far_ret(i).start()
+            else:
+                arrived(mixed_v.at[last_g, :, o], ret_r.at[last_g, o])
+            for b in range(blocks):
+                spot = slice(b * block + o * zr, b * block + (o + 1) * zr)
+                mixed = far_m[0, i, b] if zz == below else mixed_v[last_g, b, o]
+                gated_v[last_g, spot, :] = (
+                    open_v[last_g, spot, :] * mixed.astype(jnp.float32)).astype(jnp.bfloat16)
+            hand_over(last_g, o)
+
+    ends, insides = (0, zs - 1), tuple(range(1, zs - 1))
+    unit(zs - 1, 0, held_back, only=zs - 2)
+    for o in range(zs // 2):
+        unit(o, but=ends)
+    if far:
+        each_z(far_forward, lambda zz: zz == below)
     each_z(plane_round)
 
     unit(zs - 1, only=zs - 1)
+    lower = (below - 1, below)
     for o in range(zs - 1):
-        unit(o)
-        if o == 0 and held_back < groups:
-            each_d(late_mix, lambda zz: late(zz, zz + 1))
-
-    if square:
-        each_z(plane_end)
-
-    def gather_part(p):
+        if o < zs // 2:
+            unit(o, but=insides)
+        elif far and o == above:
+            unit(o, 0, last_g)
+            unit(o, last_g, groups, but=lower)
+        else:
+            unit(o)
+    if held_back < groups:
+        each_d(late_mix, lambda zz: late(zz, zz + 1))
+    if far:
+        each_z(far_above, lambda zz: zz == above)
+
+    def gather_part(g, first):
         for s in range(sp):
             @pl.when(me != s)
             def _():
-                arrived(held_v.at[s, pl.ds(p * per_part, per_part)], ga_r.at[p, s])
+                arrived(held_v.at[s, g], ga_r.at[g, s])
         squares = jnp.zeros((per, gd), jnp.float32)
         for s in range(sp):
-            for i in range(per_part):
-                g = p * per_part + i
-                value = held_v[s, g].astype(jnp.float32)
-                squares += value * value
-                cols = slice(s * chans + g * gd, s * chans + (g + 1) * gd)
-                normed_v[p, :, s * pk + i * gd:s * pk + (i + 1) * gd] = (
-                    value * ogain_ref[:, cols]).astype(jnp.bfloat16)
-        sums_v[...] = squares if p == 0 else sums_v[...] + squares
+            value = held_v[s, g].astype(jnp.float32)
+            squares += value * value
+            cols = slice(s * chans + g * gd, s * chans + (g + 1) * gd)
+            normed_v[g, :, s * pk:(s + 1) * pk] = (value * ogain_ref[:, cols]).astype(jnp.bfloat16)
+        sums_v[...] = squares if first else sums_v[...] + squares
 
     def part_dot(p, cols):
         return jnp.dot(normed_v[p], outw_v[p, :, :, cols].reshape(sp * pk, ncol),
@@ -599,27 +707,59 @@
         for r in range(1, sp):
             arrived(ow_bytes(zs - 1), pp_r.at[r])
 
-    weights_here()
-    if parts > 1:
-        unit(zs - 1, 0, groups - 1, but=zs - 1)
-        gather_part(0)
+    def plane_done():
+        if square:
+            each_z(plane_end)
+        weights_here()
+
+    started = []
+
+    def add_parts(which):
+        for g in which:
+            gather_part(g, not started)
+            started.append(g)
 
         @pl.loop(0, width // ncol)
         def _(t):
             cols = pl.ds(pl.multiple_of(t * ncol, LANES), ncol)
-            part_v[:, cols] = part_dot(0, cols)
-
-        unit(zs - 1, groups - 1, groups, but=zs - 1)
+            more = sum(part_dot(p, cols) for p in which)
+            part_v[:, cols] = more if len(started) == len(which) else part_v[:, cols] + more
+
+    done = (zs - 1, zs - 2)
+    if far:
+        unit(zs - 1, 0, last_g - 1, but=done)
+        early = (me < sp - 1) & ((z == 0) | (z == zs - 1))
+
+        def first_parts():
+            started.clear()
+            plane_done()
+            add_parts(range(last_g - 1))
+
+        pl.when(early)(first_parts)
+        each_z(far_below, lambda zz: zz in lower)
+        unit(zs - 1, last_g - 1, last_g, but=done)
+        unit(zs - 1, last_g, groups, but=lower + (zs - 1,))
+        pl.when(jnp.logical_not(early))(first_parts)
+        add_parts([last_g])
+        final = last_g - 1
+    elif groups > 1:
+        plane_done()
+        unit(zs - 1, 0, last_g, but=done)
+        add_parts(range(last_g))
+        unit(zs - 1, last_g, groups, but=(zs - 1,))
+        final = last_g
     else:
-        unit(zs - 1, but=zs - 1)
-    gather_part(parts - 1)
+        plane_done()
+        unit(zs - 1, but=done)
+        final = 0
+    gather_part(final, not started)
     scale = lax.rsqrt(jnp.sum(sums_v[...], axis=-1, keepdims=True) / (sp * chans) + norm_eps)
 
     @pl.loop(0, width // ncol)
     def _(t):
         cols = pl.ds(pl.multiple_of(t * ncol, LANES), ncol)
-        last = part_dot(parts - 1, cols)
-        if parts > 1:
+        last = part_dot(final, cols)
+        if started:
             last += part_v[:, cols]
         out_ref[:, cols] = (last * scale).astype(jnp.bfloat16)
 
@@ -642,10 +782,18 @@
                 sent(ow_bytes(n), ow_send.at[way])
         if not inner(zz):
             n = sum(v_useful(zz, q) for q in range(sp))
-            sent(norm_v.at[:, pl.ds(0, n * per), :], v_s.at[0])
+            main = pl.ds(0, last_g if split(zz) else groups)
+            sent(norm_v.at[main, pl.ds(0, n * per), :], v_s.at[0])
+            if split(zz):
+                sent(norm_v.at[pl.ds(0, 1), pl.ds(0, n * per), :], v_s.at[1])
         elif mate(zz) is not None:
             n = sum(with_mate(zz, o) for o in range(zs))
             sent(mixed_v.at[:, :, pl.ds(0, n)], ret_s.at[0])
+        for i in range(2):
+            if far and zz == below:
+                sent(far_v.at[i], fv_s.at[i])
+            if far and zz == above:
+                sent(far_m.at[:, i], fm_s.at[i])
 
     each_z(line_sent)
 
@@ -657,10 +805,13 @@
                 if not (inner(zz) or o == zz):
                     continue
                 if o >= zz and inner(zz - 1):
-                    sent(spot, mx_dn.at[o, i])
+                    crossing = last_g if far and zz == above else groups
+                    sent(mix_v.at[pl.ds(0, crossing), d, pl.ds(r0, rn), pl.ds(0, cols)],
+                         mx_dn.at[o, i])
                 if o <= zz and inner(zz + 1):
                     sent(spot, mx_up.at[o, i])
-                sent(spot, mx_ps.at[o, i])
+                paired = last_g if far and zz == below and o >= above else groups
+                sent(mix_v.at[pl.ds(0, paired), d, pl.ds(r0, rn), pl.ds(0, cols)], mx_ps.at[o, i])
 
     each_d(mix_sent)
 
@@ -672,7 +823,8 @@
     sp, dps = lax.axis_size("sp"), lax.axis_size("dp")
     zs = dps // CORES
     total = sp * per
-    parts = 1 if groups % 2 else 2
+    parts = groups
+    halves = 1 if parts % 2 else 2
     bf, f32 = jnp.bfloat16, jnp.float32
     dma = pltpu.SemaphoreType.DMA
     hbm = pl.BlockSpec(memory_space=pltpu.HBM)
@@ -697,13 +849,16 @@
             pltpu.VMEM((parts, per, sp * groups * gd // parts), bf),
             pltpu.VMEM((per, gd), f32),
             pltpu.VMEM((per, width if parts > 1 else gd), f32),
+            pltpu.VMEM((2, total if parts > 2 else 16, gd), bf),
+            pltpu.VMEM((2, 2, total // block, CORES * rows if parts > 2 else 16, gd), bf),
             dma((4,)),
             dma((zs, 2)), dma((3,)), dma((1,)),
             dma((zs,)), dma((3,)), dma((1,)), dma((2,)),
-            dma((sp,)), dma((sp, zs)), dma((1,)), dma((zs, parts)), dma((sp,)), dma((sp,)),
-            dma((groups, zs, 2)), dma((groups, zs, 2)), dma((zs, 2)), dma((zs, 2)), dma((zs, 2)),
-            dma((1,)), dma((sp, 2)), dma((1,)), dma((sp,)),
+            dma((sp,)), dma((sp, zs)), dma((1,)), dma((zs, halves)), dma((sp,)), dma((sp,)),
+            dma((groups, zs)), dma((groups, zs)), dma((zs, 2)), dma((zs, 2)), dma((zs, 2)),
+            dma((1,)), dma((sp, 2)), dma((2,)), dma((2, sp)),
             dma((1,)), dma((groups, zs)), dma((1,)), dma((parts, sp)),
+            dma((2,)), dma((2,)), dma((2,)), dma((2,)),
         ],
         compiler_params=pltpu.CompilerParams(collective_id=0, has_side_effects=True, vmem_limit_bytes=65_000_000),
     )(tokens.reshape(per, width), up_weight, gate_weight, group_gain[:, None, :], mix_weight, mix_bias,

time: 110 us -> 106 us (0.964)
  Pallas kernels: 107 us -> 104 us
    pallas_call x1, Pallas kernels: 107 us -> 104 us  [body(): pl.pallas_call(functools.partial(fused_kernel, sp, zs), out_shape=pltpu.V...]
where the time goes in v2:
time: 106 us; the launch traced here: 105 us
  Pallas kernels  104 us (98%)
  local copies, waits for them, and re-layouts  1.06 us (1%)
    pallas_call x1, Pallas kernels, body(): pl.pallas_call(functools.partial(fused_kernel, sp, zs), out_shape=pltpu.V...  104 us

profile of v2, /device:TPU:7, one launch (start us, length us, event | category | flops | bytes accessed | tf_op | source)
XLA Modules:
  0.0 105.4 jit_solution(17939619633933956788)
XLA Ops:
  0.0 104.3 %shard_map.82 = bf16[320,2048]{1,0:T(8,128)(2,1)S(1)} custom-call(bf16[320,2048]{1,0:T(8,128)(2,1)} %bitcast.6, bf16[256,2048]{1,0:T(8,128)(2,1)} %up_ref.1, bf16[256,2048]{1,0:T(8,128)(2,1)} %gate_ref.1, f32[4,1,128]{2,1,0:T(1,128)} %bitcast.9, bf16[4,160,1280]{2,1,0:T(8,128)(2,1)} %mix_ref.1, f32[4,1280]{1,0:T(4,128)} %bias_ref.1, f32[1,2048]{1,0:T(1,128)} %bitcast.8, ...), custom_call_target="tpu_custom_call" | custom-call | tf_op jit(solution)/shard_map/pallas_call | solution.py:832
  104.3 1.1 %copy.10 = bf16[1,320,2048]{2,1,0:T(8,128)(2,1)} copy(bf16[1,320,2048]{2,1,0:T(8,128)(2,1)S(1)} %bitcast.5) | data formatting | bytes 2621440

commit v3 on v2

--- a/solution.py
+++ b/solution.py
@@ -362,7 +362,8 @@
     def send_v(zz, s):
         for q in range(sp):
             if v_useful(zz, q):
-                pl.when(s == q)(lambda q=q: go(v_copies(zz, q)))
+                late_main = split(zz) and q >= sp // 2
+                pl.when(s == q)(lambda q=q, n=1 if late_main else 2: go(v_copies(zz, q)[:n]))
 
     def far_send(i, ref):
         return remote(ref.at[last_g], far_v.at[i], fv_s.at[i], fv_r.at[i], at_line(above))
@@ -404,6 +405,11 @@
                 def _():
                     arrived(tok_half(source(turn), h), tok_r.at[turn, h])
             project(source(turn))
+            if r == 1 and held_back < groups:
+                each_z(lambda zz: own_mix(zz, "dn", held_back, groups), lambda zz: zz == zs - 1)
+            if r == sp - 1:
+                for q in range(sp // 2, sp):
+                    each_z(lambda zz: go(v_copies(zz, q)[1:]), split)
 
             def events(zz, r=r):
                 first = r + 1 if inner(zz) else r
@@ -521,7 +527,7 @@
             @pl.loop(low, high)
             def _(g):
                 def rows_in(zz, cc):
-                    if not (far and zz == above and o == zs - 1 and low == last_g):
+                    if not (far and zz == above and o >= above and low == last_g):
                         arrived(mx_bytes(o * CORES + 1 - cc), mx_pr.at[g, o])
 
                 def values(at, end, spare=0):
@@ -582,9 +588,7 @@
                 hand_over(g, o)
 
     def plane_round(zz):
-        for n, o in enumerate(others(zz)):
-            if n == 1 and zz == zs - 1 and held_back < groups:
-                own_mix(zz, "dn", held_back, groups)
+        for o in others(zz):
             for r in range(1, sp):
                 if not (square and r == 3):
                     arrived(ow_piece(source(r), o, c), pl_r.at[r, o])
@@ -637,8 +641,9 @@
         for cc in range(CORES):
             @pl.when(c == cc)
             def _():
-                arrived(mx_bytes((zs - 1) * CORES + 1 - cc), mx_pr.at[last_g, zs - 1])
-        for i in range(2):
+                for o in (above, zs - 1):
+                    arrived(mx_bytes(o * CORES + 1 - cc), mx_pr.at[last_g, o])
+        for i in (1, 0):
             far_unit(i)
             far_back(i).start()
 
@@ -647,7 +652,7 @@
                       ret_s.at[0], ret_r.at[last_g, above + i], at_line(below - 1))
 
     def far_below(zz):
-        for i in range(2):
+        for i in (1, 0):
             o = above + i
             if zz == below:
                 arrived(far_m.at[:, i], fm_r.at[i])
@@ -675,14 +680,14 @@
         if o < zs // 2:
             unit(o, but=insides)
         elif far and o == above:
+            each_d(late_mix, lambda zz: late(zz, zz + 1))
+            each_z(far_above, lambda zz: zz == above)
             unit(o, 0, last_g)
             unit(o, last_g, groups, but=lower)
         else:
             unit(o)
-    if held_back < groups:
+    if held_back < groups and not far:
         each_d(late_mix, lambda zz: late(zz, zz + 1))
-    if far:
-        each_z(far_above, lambda zz: zz == above)
 
     def gather_part(g, first):
         for s in range(sp):
@@ -697,8 +702,10 @@
             normed_v[g, :, s * pk:(s + 1) * pk] = (value * ogain_ref[:, cols]).astype(jnp.bfloat16)
         sums_v[...] = squares if first else sums_v[...] + squares
 
+    step = 2 * ncol if width % (2 * ncol) == 0 else ncol
+
     def part_dot(p, cols):
-        return jnp.dot(normed_v[p], outw_v[p, :, :, cols].reshape(sp * pk, ncol),
+        return jnp.dot(normed_v[p], outw_v[p, :, :, cols].reshape(sp * pk, step),
                        preferred_element_type=jnp.float32)
 
     def weights_here():
@@ -707,11 +714,6 @@
         for r in range(1, sp):
             arrived(ow_bytes(zs - 1), pp_r.at[r])
 
-    def plane_done():
-        if square:
-            each_z(plane_end)
-        weights_here()
-
     started = []
 
     def add_parts(which):
@@ -719,9 +721,9 @@
             gather_part(g, not started)
             started.append(g)
 
-        @pl.loop(0, width // ncol)
+        @pl.loop(0, width // step)
         def _(t):
-            cols = pl.ds(pl.multiple_of(t * ncol, LANES), ncol)
+            cols = pl.ds(pl.multiple_of(t * step, LANES), step)
             more = sum(part_dot(p, cols) for p in which)
             part_v[:, cols] = more if len(started) == len(which) else part_v[:, cols] + more
 
@@ -732,9 +734,11 @@
 
         def first_parts():
             started.clear()
-            plane_done()
+            weights_here()
             add_parts(range(last_g - 1))
 
+        if square:
+            each_z(plane_end)
         pl.when(early)(first_parts)
         each_z(far_below, lambda zz: zz in lower)
         unit(zs - 1, last_g - 1, last_g, but=done)
@@ -743,21 +747,25 @@
         add_parts([last_g])
         final = last_g - 1
     elif groups > 1:
-        plane_done()
+        if square:
+            each_z(plane_end)
+        weights_here()
         unit(zs - 1, 0, last_g, but=done)
         add_parts(range(last_g))
         unit(zs - 1, last_g, groups, but=(zs - 1,))
         final = last_g
     else:
-        plane_done()
+        if square:
+            each_z(plane_end)
+        weights_here()
         unit(zs - 1, but=done)
         final = 0
     gather_part(final, not started)
     scale = lax.rsqrt(jnp.sum(sums_v[...], axis=-1, keepdims=True) / (sp * chans) + norm_eps)
 
-    @pl.loop(0, width // ncol)
+    @pl.loop(0, width // step)
     def _(t):
-        cols = pl.ds(pl.multiple_of(t * ncol, LANES), ncol)
+        cols = pl.ds(pl.multiple_of(t * step, LANES), step)
         last = part_dot(final, cols)
         if started:
             last += part_v[:, cols]

time: 106 us -> 103 us (0.972)
  Pallas kernels: 104 us -> 101 us
    pallas_call x1, Pallas kernels: 104 us -> 101 us  [body(): pl.pallas_call(functools.partial(fused_kernel, sp, zs), out_shape=pltpu.V...]
where the time goes in v3:
time: 103 us; the launch traced here: 102 us
  Pallas kernels  101 us (98%)
  local copies, waits for them, and re-layouts  1.06 us (1%)
    pallas_call x1, Pallas kernels, body(): pl.pallas_call(functools.partial(fused_kernel, sp, zs), out_shape=pltpu.V...  101 us

profile of v3, /device:TPU:7, one launch (start us, length us, event | category | flops | bytes accessed | tf_op | source)
XLA Modules:
  0.0 102.4 jit_solution(17278066866938349171)
XLA Ops:
  0.0 101.3 %shard_map.82 = bf16[320,2048]{1,0:T(8,128)(2,1)S(1)} custom-call(bf16[320,2048]{1,0:T(8,128)(2,1)} %bitcast.6, bf16[256,2048]{1,0:T(8,128)(2,1)} %up_ref.1, bf16[256,2048]{1,0:T(8,128)(2,1)} %gate_ref.1, f32[4,1,128]{2,1,0:T(1,128)} %bitcast.9, bf16[4,160,1280]{2,1,0:T(8,128)(2,1)} %mix_ref.1, f32[4,1280]{1,0:T(4,128)} %bias_ref.1, f32[1,2048]{1,0:T(1,128)} %bitcast.8, ...), custom_call_target="tpu_custom_call" | custom-call | tf_op jit(solution)/shard_map/pallas_call | solution.py:840
  101.3 1.1 %copy.10 = bf16[1,320,2048]{2,1,0:T(8,128)(2,1)} copy(bf16[1,320,2048]{2,1,0:T(8,128)(2,1)S(1)} %bitcast.5) | data formatting | bytes 2621440

commit v4 on v3

--- a/solution.py
+++ b/solution.py
@@ -698,11 +698,11 @@
         for s in range(sp):
             value = held_v[s, g].astype(jnp.float32)
             squares += value * value
-            cols = slice(s * chans + g * gd, s * chans + (g + 1) * gd)
+            cols = pl.ds(pl.multiple_of(s * chans + g * gd, LANES), gd)
             normed_v[g, :, s * pk:(s + 1) * pk] = (value * ogain_ref[:, cols]).astype(jnp.bfloat16)
         sums_v[...] = squares if first else sums_v[...] + squares
 
-    step = 2 * ncol if width % (2 * ncol) == 0 else ncol
+    step = 4 * ncol if width % (4 * ncol) == 0 else ncol
 
     def part_dot(p, cols):
         return jnp.dot(normed_v[p], outw_v[p, :, :, cols].reshape(sp * pk, step),
@@ -730,7 +730,7 @@
     done = (zs - 1, zs - 2)
     if far:
         unit(zs - 1, 0, last_g - 1, but=done)
-        early = (me < sp - 1) & ((z == 0) | (z == zs - 1))
+        early = (z == 0) & (me < sp // 2)
 
         def first_parts():
             started.clear()
@@ -744,8 +744,8 @@
         unit(zs - 1, last_g - 1, last_g, but=done)
         unit(zs - 1, last_g, groups, but=lower + (zs - 1,))
         pl.when(jnp.logical_not(early))(first_parts)
-        add_parts([last_g])
-        final = last_g - 1
+        final = jnp.where(me == sp - 1, last_g - 1, last_g)
+        add_parts([2 * last_g - 1 - final])
     elif groups > 1:
         if square:
             each_z(plane_end)

time: 103 us -> 102 us (level)
  no operation moved by 1% of the time
where the time goes in v4:
time: 102 us
  Pallas kernels  101 us (99%)
  local copies, waits for them, and re-layouts  1.06 us (1%)
    pallas_call x1, Pallas kernels, body(): pl.pallas_call(functools.partial(fused_kernel, sp, zs), out_shape=pltpu.V...  101 us

profile of v4, /device:TPU:7, one launch (start us, length us, event | category | flops | bytes accessed | tf_op | source)
XLA Modules:
  0.0 102.0 jit_solution(16265061766884283242)
XLA Ops:
  0.0 101.0 %shard_map.82 = bf16[320,2048]{1,0:T(8,128)(2,1)S(1)} custom-call(bf16[320,2048]{1,0:T(8,128)(2,1)} %bitcast.6, bf16[256,2048]{1,0:T(8,128)(2,1)} %up_ref.1, bf16[256,2048]{1,0:T(8,128)(2,1)} %gate_ref.1, f32[4,1,128]{2,1,0:T(1,128)} %bitcast.9, bf16[4,160,1280]{2,1,0:T(8,128)(2,1)} %mix_ref.1, f32[4,1280]{1,0:T(4,128)} %bias_ref.1, f32[1,2048]{1,0:T(1,128)} %bitcast.8, ...), custom_call_target="tpu_custom_call" | custom-call | tf_op jit(solution)/shard_map/pallas_call | solution.py:840
  101.0 1.1 %copy.10 = bf16[1,320,2048]{2,1,0:T(8,128)(2,1)} copy(bf16[1,320,2048]{2,1,0:T(8,128)(2,1)S(1)} %bitcast.5) | data formatting | bytes 2621440

commit v5 on v4

--- a/solution.py
+++ b/solution.py
@@ -702,7 +702,7 @@
             normed_v[g, :, s * pk:(s + 1) * pk] = (value * ogain_ref[:, cols]).astype(jnp.bfloat16)
         sums_v[...] = squares if first else sums_v[...] + squares
 
-    step = 4 * ncol if width % (4 * ncol) == 0 else ncol
+    step = 8 * ncol if width % (8 * ncol) == 0 else ncol
 
     def part_dot(p, cols):
         return jnp.dot(normed_v[p], outw_v[p, :, :, cols].reshape(sp * pk, step),

time: 102 us -> 102 us (level)
  no operation moved by 1% of the time
where the time goes in v5:
time: 102 us
  Pallas kernels  101 us (99%)
  local copies, waits for them, and re-layouts  1.06 us (1%)
    pallas_call x1, Pallas kernels, body(): pl.pallas_call(functools.partial(fused_kernel, sp, zs), out_shape=pltpu.V...  101 us

profile of v5, /device:TPU:7, one launch (start us, length us, event | category | flops | bytes accessed | tf_op | source)
XLA Modules:
  0.0 101.7 jit_solution(7498269088344438252)
XLA Ops:
  0.0 100.6 %shard_map.82 = bf16[320,2048]{1,0:T(8,128)(2,1)S(1)} custom-call(bf16[320,2048]{1,0:T(8,128)(2,1)} %bitcast.6, bf16[256,2048]{1,0:T(8,128)(2,1)} %up_ref.1, bf16[256,2048]{1,0:T(8,128)(2,1)} %gate_ref.1, f32[4,1,128]{2,1,0:T(1,128)} %bitcast.9, bf16[4,160,1280]{2,1,0:T(8,128)(2,1)} %mix_ref.1, f32[4,1280]{1,0:T(4,128)} %bias_ref.1, f32[1,2048]{1,0:T(1,128)} %bitcast.8, ...), custom_call_target="tpu_custom_call" | custom-call | tf_op jit(solution)/shard_map/pallas_call | solution.py:840
  100.6 1.1 %copy.10 = bf16[1,320,2048]{2,1,0:T(8,128)(2,1)} copy(bf16[1,320,2048]{2,1,0:T(8,128)(2,1)S(1)} %bitcast.5) | data formatting | bytes 2621440
